TPU v7x, 512 devices: a whole 4x4x16 slice. The times are simulated.
512 devices in a mesh: fs: 64 (over z, y), tp: 8 (over x, core).
Axes of the slice: x: 4, y: 4, z: 16, core: 2. Of those that a mesh axis runs over, the one named last changes fastest.
Arguments:
- block_input: bfloat16 [65536, 2048], P('fs'), may hold values from -6 to 6
- value_cotangent: bfloat16 [65536, 1024], P('fs', 'tp'), may hold values from -6 to 6
- mixed_output: bfloat16 [65536, 1024], P('fs', 'tp'), may hold values from -6 to 6
- output_cotangent: bfloat16 [65536, 2048], P('fs'), may hold values from -6 to 6
- value_weight: float32 [2048, 1024], P('fs', 'tp'), may hold values from -0.125 to 0.125
- output_weight: float32 [1024, 2048], P('tp', 'fs'), may hold values from -0.1875 to 0.1875
- value_basis: bfloat16 [2048, 384], P('fs'), may hold values from -0.125 to 0.125
- output_basis: bfloat16 [2048, 384], P('fs'), may hold values from -0.125 to 0.125
- value_mean: float32 [384, 1024], P(None, 'tp'), may hold values from -4 to 4
- value_square: float32 [384, 1024], P(None, 'tp'), may hold values from 0.3 to 2
- output_mean: float32 [1024, 384], P('tp'), may hold values from -4 to 4
- output_square: float32 [1024, 384], P('tp'), may hold values from 0.3 to 2
Outputs:
- value_next: float32 [2048, 1024], P('fs', 'tp')
- value_copy: bfloat16 [2048, 1024], P(None, 'tp')
- value_step: float32 [2048, 1024], P('fs', 'tp')
- value_mean_next: float32 [384, 1024], P(None, 'tp')
- value_square_next: float32 [384, 1024], P(None, 'tp')
- output_next: float32 [1024, 2048], P('tp', 'fs')
- output_copy: bfloat16 [1024, 2048], P('tp')
- output_step: float32 [1024, 2048], P('tp', 'fs')
- output_mean_next: float32 [1024, 384], P('tp')
- output_square_next: float32 [1024, 384], P('tp')
All inputs are finite; a program needn't handle non-finite values.
Results may differ from a plain program's by a relative error of at most 0.002.
Values may be sent and summed in bfloat16 or wider, within the bound.
A program may use at most 64 MiB of HBM per device.

v0:
```python
import math

import jax
import jax.numpy as jnp
from jax import lax
from jax.sharding import Mesh
from jax.sharding import PartitionSpec as P

FS = ("fs_0", "fs_1")


def own_block(parts, axes, turns):
    shape = [lax.axis_size(a) for a in axes]
    parts = parts.reshape(*shape, *parts.shape[1:])
    parts = parts.transpose(*turns, *range(len(axes), parts.ndim))
    parts = parts.reshape(-1, *parts.shape[len(axes) :])
    for k in turns:
        parts = lax.psum_scatter(parts, axes[k], scatter_dimension=0, tiled=True)
    return parts[0]


def cut_along(shard, dim, size):
    before, after = (shard.shape[:dim], shard.shape[dim + 1 :])
    return jnp.moveaxis(shard.reshape(*before, size, -1, *after), dim, 0)


def summed_rows(shard, axes, turns, dim):
    size = lax.axis_size(axes)
    return own_block(cut_along(shard, dim, size), axes, turns)


def together(arrays, axis):
    flat, at, done = (jnp.concatenate([a.reshape(-1) for a in arrays]), 0, [])
    so_far = lax.psum(flat, axis)
    for a in arrays:
        done.append(so_far[at : at + a.size].reshape(a.shape))
        at += a.size
    return tuple(done)


def from_everyone(shard, axis):
    copies = jnp.broadcast_to(shard, (lax.axis_size(axis), *shard.shape))
    return lax.all_to_all(copies, axis, split_axis=0, concat_axis=0, tiled=True)


def of_everyone(shard, axis):
    return from_everyone(shard, axis).sum(axis=0)


def packed_total(arrays, axis):
    flat, at, done = (jnp.concatenate([a.reshape(-1) for a in arrays]), 0, [])
    so_far = of_everyone(flat, axis)
    for a in arrays:
        done.append(so_far[at : at + a.size].reshape(a.shape))
        at += a.size
    return tuple(done)


def joined_along(parts, dim):
    parts = jnp.moveaxis(parts, 0, dim)
    shape = parts.shape
    return parts.reshape(*shape[:dim], shape[dim] * shape[dim + 1], *shape[dim + 2 :])


def gather_directly(shard, axis, dim):
    return joined_along(from_everyone(shard, axis), dim)


def on_device(
    block_input,
    value_cotangent,
    mixed_output,
    output_cotangent,
    value_weight,
    output_weight,
    value_basis,
    output_basis,
    value_mean,
    value_square,
    output_mean,
    output_square,
):
    highest = lax.Precision.HIGHEST
    tokens_all = block_input.shape[0] * lax.axis_size(FS)
    scaling = 1.0 / math.sqrt(tokens_all)
    rank_size = value_basis.shape[1]
    local_width = value_cotangent.shape[1]
    contract = (((0,), (0,)), ((), ()))
    value_grad = lax.dot_general(
        block_input, value_cotangent, contract, preferred_element_type=jnp.float32
    )
    output_grad = lax.dot_general(
        output_cotangent, mixed_output, contract, preferred_element_type=jnp.float32
    )
    summed = summed_rows(jnp.concatenate([value_grad, output_grad], axis=1), FS, (1, 0), 0)
    value_part = jnp.dot(
        value_basis.astype(jnp.float32).T, summed[:, :local_width], precision=highest
    )
    output_part = jnp.dot(
        summed[:, local_width:].T, output_basis.astype(jnp.float32), precision=highest
    )
    value_low, output_low = together((value_part * scaling, output_part * scaling), FS)
    value_squares, output_squares = packed_total(
        (jnp.sum(value_low * value_low), jnp.sum(output_low * output_low)), "tp"
    )
    entries = 2.0 * rank_size * local_width * lax.axis_size("tp")
    clip_scale = 1.0 / jnp.sqrt(1.0 + (value_squares + output_squares) / entries)
    value_scaled = clip_scale * value_low
    output_scaled = clip_scale * output_low
    value_mean_next = 0.8 * value_mean + 0.2 * value_scaled
    output_mean_next = 0.8 * output_mean + 0.2 * output_scaled
    value_square_next = 0.9 * value_square + 0.1 * value_scaled * value_scaled
    output_square_next = 0.9 * output_square + 0.1 * output_scaled * output_scaled
    value_norm = value_mean_next / jnp.sqrt(value_square_next + 0.1)
    output_norm = output_mean_next / jnp.sqrt(output_square_next + 0.1)
    value_step = jnp.dot(value_basis.astype(jnp.float32), value_norm, precision=highest)
    output_step = jnp.dot(output_norm, output_basis.astype(jnp.float32).T, precision=highest)
    value_next = value_weight - 0.02 * value_step
    output_next = output_weight - 0.02 * output_step
    value_copy = gather_directly(value_next.astype(jnp.bfloat16), FS, 0)
    output_copy = gather_directly(output_next.astype(jnp.bfloat16), FS, 1)
    return (
        value_next,
        value_copy,
        value_step,
        value_mean_next,
        value_square_next,
        output_next,
        output_copy,
        output_step,
        output_mean_next,
        output_square_next,
    )


def solution(mesh):
    torus = Mesh(mesh.devices.reshape(16, 4, mesh.shape["tp"]), ("fs_0", "fs_1", "tp"))
    placed = (
        P(FS, None),
        P(FS, "tp"),
        P(FS, "tp"),
        P(FS, None),
        P(FS, "tp"),
        P("tp", FS),
        P(FS, None),
        P(FS, None),
        P(None, "tp"),
        P(None, "tp"),
        P("tp", None),
        P("tp", None),
    )
    return jax.shard_map(
        on_device,
        mesh=torus,
        in_specs=placed,
        out_specs=(
            P(FS, "tp"),
            P(None, "tp"),
            P(FS, "tp"),
            P(None, "tp"),
            P(None, "tp"),
            P("tp", FS),
            P("tp", None),
            P("tp", FS),
            P("tp", None),
            P("tp", None),
        ),
        check_vma=False,
    )
```

profile of v0, /device:TPU:1, one launch (start us, length us, event | category | flops | bytes accessed | tf_op | source)
XLA Modules:
  0.0 503.9 jit_solution(17562238249384993903)
XLA Ops:
  7.2 0.0 copy-start
  7.2 0.0 reduce-scatter.3.cloned.1.call-start
  7.2 0.9 copy-done
  8.1 3.1 fusion.20
  11.2 0.4 copy-done.1
  11.6 0.8 fusion.21
  12.4 0.1 pad_maximum_fusion
  12.5 1.9 copy.31
  14.4 3.2 copy.32
  17.6 0.0 copy-start.9
  17.6 0.0 reduce-scatter.3.cloned.1.call-update
  17.6 0.0 copy-start.15
  17.6 0.0 reduce-scatter.5.cloned.1.call-start
  17.7 42.7 %reduce-scatter.3.cloned.1.call-done = f32[16,32,256]{2,1,0:T(8,128)} async-done(((f32[64,32,256]{2,1,0:T(8,128)}), f32[16,32,256]{2,1,0:T(8,128)}) %reduce-scatter.3.cloned.1.call-update) | async-done | bytes 524304 | tf_op jit(solution)/shard_map/reduce_scatter | solution.py:18
  60.4 0.0 reduce-scatter.5.cloned.1.call-update
  60.4 0.0 all-reduce.2.cloned.1.call-start
  60.5 61.6 %reduce-scatter.5.cloned.1.call-done = f32[1,32,256]{2,1,0:T(8,128)} async-done(((f32[16,32,256]{2,1,0:T(8,128)}), f32[1,32,256]{2,1,0:T(8,128)}) %reduce-scatter.5.cloned.1.call-update) | async-done | bytes 32784 | tf_op jit(solution)/shard_map/reduce_scatter | solution.py:18
  122.0 0.0 copy-done.12
  122.0 1.0 convolution_multiply_fusion
  123.1 0.0 copy-done.13
  123.1 1.0 fusion
  124.1 0.1 copy.33
  124.2 0.8 pad_maximum_fusion.1
  125.0 0.0 all-reduce.2.cloned.1.call-update
  125.0 267.9 %all-reduce.2.cloned.1.call-done = f32[98304]{0:T(1024)} async-done(((f32[98304]{0:T(1024)}), f32[98304]{0:T(1024)}) %all-reduce.2.cloned.1.call-update) | async-done | bytes 393232 | tf_op jit(solution)/shard_map/psum | solution.py:34
  392.9 1.7 multiply_reduce_fusion.1
  394.6 1.4 pad_maximum_fusion.2
  396.0 19.3 %all_to_all.16 = f32[8,1,2]{2,1,0:T(1,128)S(1)} all-to-all(f32[8,1,2]{2,1,0:T(1,128)S(1)} %broadcast_in_dim.9), channel_id=1, replica_groups=mesh['fs_0'=16,'fs_1'=4,'tp'=8] {'tp'}, dimensions={0} | all-to-all | bytes 128 | tf_op jit(solution)/shard_map/all_to_all | solution.py:43
  415.3 0.6 fusion.19
  417.3 0.9 slice_multiply_fusion
  418.3 0.1 fusion.2
  418.4 0.0 copy-start.5
  418.4 0.0 copy-start.6
  418.4 0.0 copy-done.14
  418.4 0.9 fusion.17
  419.3 0.9 broadcast_in_dim.11
  420.1 8.3 %all-to-all-start.2 = ((bf16[64,128,32]{1,2,0:T(8,128)(2,1)}), bf16[64,128,32]{1,2,0:T(8,128)(2,1)S(1)}, u32[]{:S(2)}, u32[]{:S(2)}) async-start(bf16[64,128,32]{1,2,0:T(8,128)(2,1)} %broadcast_in_dim.11), calls=%async_computation.4 | async-start | bytes 1048576 | tf_op jit(solution)/shard_map/all_to_all | solution.py:43
  428.4 0.0 copy-done.8
  428.5 0.1 fusion.1
  428.5 0.0 copy-start.3
  428.5 0.0 copy-start.4
  428.6 0.8 fusion.18
  429.4 29.9 %all-to-all-done.2 = bf16[64,128,32]{1,2,0:T(8,128)(2,1)S(1)} async-done(((bf16[64,128,32]{1,2,0:T(8,128)(2,1)}), bf16[64,128,32]{1,2,0:T(8,128)(2,1)S(1)}, u32[]{:S(2)}, u32[]{:S(2)}) %all-to-all-start.2) | async-done | bytes 524320 | tf_op jit(solution)/shard_map/all_to_all | solution.py:43
  459.3 0.9 broadcast_in_dim.10
  460.2 7.0 %all-to-all-start.1 = ((bf16[64,32,128]{2,1,0:T(8,128)(2,1)}), bf16[64,32,128]{2,1,0:T(8,128)(2,1)S(1)}, u32[]{:S(2)}, u32[]{:S(2)}) async-start(bf16[64,32,128]{2,1,0:T(8,128)(2,1)} %broadcast_in_dim.10), calls=%async_computation.3 | async-start | bytes 1048576 | tf_op jit(solution)/shard_map/all_to_all | solution.py:43
  467.2 1.0 copy.35
  468.2 28.3 %all-to-all-done.1 = bf16[64,32,128]{2,1,0:T(8,128)(2,1)S(1)} async-done(((bf16[64,32,128]{2,1,0:T(8,128)(2,1)}), bf16[64,32,128]{2,1,0:T(8,128)(2,1)S(1)}, u32[]{:S(2)}, u32[]{:S(2)}) %all-to-all-start.1) | async-done | bytes 524320 | tf_op jit(solution)/shard_map/all_to_all | solution.py:43
  496.5 0.8 copy.41
  (23 shorter events, 0.1 us)
Async XLA Ops:
  7.2 1.0 copy-start
  7.2 4.0 copy-start.7
  7.2 53.2 %reduce-scatter.3.cloned.1.call-start = ((), (), s32[]{:S(2)}) async-start(), calls=%async_computation.5 | async-start | bytes 2621440 | tf_op jit(solution)/shard_map/reduce_scatter | solution.py:18
  8.1 3.5 copy-start.1
  14.4 107.7 %copy-start.12 = (bf16[32,384]{1,0:T(8,128)(2,1)S(1)}, bf16[32,384]{1,0:T(8,128)(2,1)}, u32[]{:S(2)}) copy-start(bf16[32,384]{1,0:T(8,128)(2,1)} %param.19) | copy-start | bytes 73732
  14.4 108.7 %copy-start.13 = (bf16[32,384]{1,0:T(8,128)(2,1)S(1)}, bf16[32,384]{1,0:T(8,128)(2,1)}, u32[]{:S(2)}) copy-start(bf16[32,384]{1,0:T(8,128)(2,1)} %param.18) | copy-start | bytes 73732
  17.6 400.7 %copy-start.10 = (f32[128,384]{1,0:T(8,128)S(1)}, f32[128,384]{1,0:T(8,128)}, u32[]{:S(2)}) copy-start(f32[128,384]{1,0:T(8,128)} %param.23) | copy-start | bytes 589828
  17.6 400.7 %copy-start.11 = (f32[128,384]{1,0:T(8,128)S(1)}, f32[128,384]{1,0:T(8,128)}, u32[]{:S(2)}) copy-start(f32[128,384]{1,0:T(8,128)} %param.22) | copy-start | bytes 589828
  17.6 400.8 %copy-start.14 = (f32[128,32]{0,1:T(8,128)S(1)}, f32[128,32]{0,1:T(8,128)}, u32[]{:S(2)}) copy-start(f32[128,32]{0,1:T(8,128)} %param.17) | copy-start | bytes 49156
  17.6 410.8 %copy-start.8 = (f32[384,128]{1,0:T(8,128)S(1)}, f32[384,128]{1,0:T(8,128)}, u32[]{:S(2)}) copy-start(f32[384,128]{1,0:T(8,128)} %param.21) | copy-start | bytes 589828
  17.6 410.8 %copy-start.9 = (f32[384,128]{1,0:T(8,128)S(1)}, f32[384,128]{1,0:T(8,128)}, u32[]{:S(2)}) copy-start(f32[384,128]{1,0:T(8,128)} %param.20) | copy-start | bytes 589828
  17.6 410.9 %copy-start.15 = (f32[32,128]{1,0:T(8,128)S(1)}, f32[32,128]{1,0:T(8,128)}, u32[]{:S(2)}) copy-start(f32[32,128]{1,0:T(8,128)} %param.16) | copy-start | bytes 49156
  17.6 104.4 %reduce-scatter.5.cloned.1.call-start = ((), (), s32[]{:S(2)}) async-start(), calls=%async_computation.6 | async-start | bytes 557056 | tf_op jit(solution)/shard_map/reduce_scatter | solution.py:18
  60.4 332.5 %all-reduce.2.cloned.1.call-start = ((), (), s32[]{:S(2)}) async-start(), calls=%async_computation.7 | async-start | bytes 786432 | tf_op jit(solution)/shard_map/psum | solution.py:34
  392.9 35.6 %copy-start.2 = (f32[98304]{0:T(1024)S(1)}, f32[98304]{0:T(1024)}, u32[]{:S(2)}) copy-start(f32[98304]{0:T(1024)} %all-reduce.2.cloned.1.call-done) | copy-start | bytes 1179652
  418.4 79.0 %copy-start.5 = (f32[128,384]{1,0:T(8,128)}, f32[128,384]{1,0:T(8,128)S(1)}, u32[]{:S(2)}) copy-start(f32[128,384]{1,0:T(8,128)S(1)} %get-tuple-element.73) | copy-start | bytes 589828
  418.4 78.9 %copy-start.6 = (f32[128,384]{1,0:T(8,128)}, f32[128,384]{1,0:T(8,128)S(1)}, u32[]{:S(2)}) copy-start(f32[128,384]{1,0:T(8,128)S(1)} %get-tuple-element.72) | copy-start | bytes 589828
  420.1 39.2 %all-to-all-start.2 = ((bf16[64,128,32]{1,2,0:T(8,128)(2,1)}), bf16[64,128,32]{1,2,0:T(8,128)(2,1)S(1)}, u32[]{:S(2)}, u32[]{:S(2)}) async-start(bf16[64,128,32]{1,2,0:T(8,128)(2,1)} %broadcast_in_dim.11), calls=%async_computation.4 | async-start | bytes 1048576 | tf_op jit(solution)/shard_map/all_to_all | solution.py:43
  428.5 68.8 %copy-start.3 = (f32[384,128]{1,0:T(8,128)}, f32[384,128]{1,0:T(8,128)S(1)}, u32[]{:S(2)}) copy-start(f32[384,128]{1,0:T(8,128)S(1)} %get-tuple-element.68) | copy-start | bytes 589828
  428.5 68.8 %copy-start.4 = (f32[384,128]{1,0:T(8,128)}, f32[384,128]{1,0:T(8,128)S(1)}, u32[]{:S(2)}) copy-start(f32[384,128]{1,0:T(8,128)S(1)} %get-tuple-element.67) | copy-start | bytes 589828
  460.2 36.3 %all-to-all-start.1 = ((bf16[64,32,128]{2,1,0:T(8,128)(2,1)}), bf16[64,32,128]{2,1,0:T(8,128)(2,1)S(1)}, u32[]{:S(2)}, u32[]{:S(2)}) async-start(bf16[64,32,128]{2,1,0:T(8,128)(2,1)} %broadcast_in_dim.10), calls=%async_computation.3 | async-start | bytes 1048576 | tf_op jit(solution)/shard_map/all_to_all | solution.py:43
Sparse Core Ops, SparseCore 0:
  17.7 42.6 reduce-scatter.2
  63.2 58.7 reduce-scatter.4
  126.0 266.8 all-reduce.1
where the time goes:
time: 507 us; the launch traced here: 504 us
  waiting for transfers between devices  430 us (85%)
  blocking collectives  19.3 us (4%)
  between operations  15.4 us (3%)
  starting transfers between devices  15.3 us (3%)
  local copies, waits for them, and re-layouts  10.7 us (2%)
  matrix products  7.61 us (2%)
  other arithmetic  5.1 us (1%)
    psum x1, waiting for transfers between devices, together(): so_far = lax.psum(flat, axis)  268 us
    reduce_scatter x2, waiting for transfers between devices, own_block(): parts = lax.psum_scatter(parts, axes[k], scatter_dimension=0, tiled=True)  104 us
    all_to_all x2, waiting for transfers between devices, from_everyone(): return lax.all_to_all(copies, axis, split_axis=0, concat_axis=0, tiled=True)  58.3 us
    all_to_all x1, blocking collectives, from_everyone(): return lax.all_to_all(copies, axis, split_axis=0, concat_axis=0, tiled=True)  19.3 us
    all_to_all x2, starting transfers between devices, from_everyone(): return lax.all_to_all(copies, axis, split_axis=0, concat_axis=0, tiled=True)  15.2 us
  transfers between devices with their start and end apart: 5, of which 5 were waited for; matrix products, arithmetic and copies ran while one was open for 0% of the time, Pallas kernels for 0%

commit v1 on v0

v1 whole, which is shorter than its diff:
```python
import functools
import math

import jax
import jax.numpy as jnp
from jax import lax
from jax.experimental import pallas as pl
from jax.experimental.pallas import tpu as pltpu
from jax.sharding import PartitionSpec as P

NZ, NY, NX, NC = 16, 4, 4, 2
MESH = pl.DeviceIdType.MESH
W_BOUND = 0.1875
W_SLOPE = 250.0 / W_BOUND
CHUNKS = 4
FAR_FIRST = (8, 7, 9, 6, 10, 5, 11, 4, 12, 3, 13, 2, 14, 1, 15)


def coded(weight):
    size = jnp.exp2(jnp.abs(weight) * W_SLOPE - 125.0)
    return jnp.where(weight < 0, -size, size).astype(jnp.bfloat16)


def decoded(code):
    code = code.astype(jnp.float32)
    size = (jnp.log2(jnp.abs(code)) + 125.0) * (1.0 / W_SLOPE)
    return jnp.where(code < 0, -size, size)


def kernel(
    scaling,
    entries,
    x_hbm,
    v_hbm,
    m_hbm,
    oc_hbm,
    vb_hbm,
    ob_hbm,
    w_hbm,
    vmean_hbm,
    vsq_hbm,
    omean_hbm,
    osq_hbm,
    vmean_out,
    vsq_out,
    omean_out,
    osq_out,
    vcopy_out,
    ocopy_out,
    own_out,
    xs,
    ocs,
    vs,
    ms,
    shard,
    basis,
    weights,
    grads,
    ysend,
    yrecv,
    zsend,
    zrecv,
    lows,
    sums,
    small,
    vstate,
    ostate,
    load_sem,
    chunk_sem,
    bz_s,
    bz_r,
    by_s,
    by_r,
    bx_s,
    bx_r,
    bd_s,
    bd_r,
    ry_s,
    ry_r,
    rz_s,
    rz_r,
    az_s,
    az_r,
    ay_s,
    ay_r,
    cl_s,
    cl_r,
    wz_s,
    wz_r,
    wy_s,
    wy_r,
):
    fs, tp = lax.axis_index("fs"), lax.axis_index("tp")
    z, y = fs // NY, lax.rem(fs, NY)
    x, c = tp // NC, lax.rem(tp, NC)
    parity = lax.rem(x, 2)
    tokens, width = xs.shape
    rank = basis.shape[3]
    local = vs.shape[1]
    rows = basis.shape[2]

    def zdev(zz):
        return {"fs": zz * NY + y, "tp": tp}

    def ydev(yy):
        return {"fs": z * NY + yy, "tp": tp}

    def xdev(xx):
        return {"fs": fs, "tp": xx * NC + c}

    sibling = {"fs": fs, "tp": x * NC + 1 - c}

    def zup(j):
        return lax.rem(z + j, NZ)

    def yup(j):
        return lax.rem(y + j, NY)

    def xup(j):
        return lax.rem(x + j, NX)

    def remote(src, dst, ssem, rsem, device):
        return pltpu.make_async_remote_copy(
            src_ref=src, dst_ref=dst, send_sem=ssem, recv_sem=rsem, device_id=device, device_id_type=MESH
        )

    here = y * (NX * NC) + tp

    def plane(j):
        other = lax.rem(here + j, NY * NX * NC)
        return {"fs": z * NY + other // (NX * NC), "tp": lax.rem(other, NX * NC)}

    for k, far in enumerate((vb_hbm, ob_hbm)):

        @pl.when(c == k)
        def _(k=k, far=far):
            pltpu.make_async_copy(far, shard, load_sem.at[0]).start()

            @pl.when(parity == 0)
            def _():
                pltpu.make_async_copy(far, basis.at[k, fs], load_sem.at[1]).start()

    pltpu.make_async_copy(v_hbm, vs, load_sem.at[2]).start()
    pltpu.make_async_copy(m_hbm, ms, load_sem.at[3]).start()
    size = tokens // CHUNKS
    for t in range(CHUNKS):
        at = pl.ds(t * size, size)
        pltpu.make_async_copy(x_hbm.at[at], xs.at[at], chunk_sem.at[0, t]).start()
        pltpu.make_async_copy(oc_hbm.at[at], ocs.at[at], chunk_sem.at[1, t]).start()
    pltpu.make_async_copy(vmean_hbm, vstate.at[0], load_sem.at[4]).start()
    pltpu.make_async_copy(vsq_hbm, vstate.at[1], load_sem.at[5]).start()
    pltpu.make_async_copy(omean_hbm, ostate.at[0], load_sem.at[6]).start()
    pltpu.make_async_copy(osq_hbm, ostate.at[1], load_sem.at[7]).start()
    pltpu.make_async_copy(w_hbm, weights.at[fs], load_sem.at[8]).start()

    barrier = pltpu.get_barrier_semaphore()
    for j in range(1, NZ):
        pl.semaphore_signal(barrier, inc=1, device_id=zdev(zup(j)), device_id_type=MESH)
    for j in range(1, NY * NX * NC):
        pl.semaphore_signal(barrier, inc=1, device_id=plane(j), device_id_type=MESH)

    pltpu.make_async_copy(v_hbm, vs, load_sem.at[2]).wait()
    pltpu.make_async_copy(m_hbm, ms, load_sem.at[3]).wait()
    across = (((0,), (0,)), ((), ()))
    for t in range(CHUNKS):
        at = pl.ds(t * size, size)
        for k, (far, near, thin) in enumerate(((x_hbm, xs, vs), (oc_hbm, ocs, ms))):
            pltpu.make_async_copy(far.at[at], near.at[at], chunk_sem.at[k, t]).wait()
            part = lax.dot_general(thin[at, :], near[at, :], across, preferred_element_type=jnp.float32)
            if t == 0:
                grads[k] = part
            else:
                grads[k] += part

    pltpu.make_async_copy(vb_hbm, shard, load_sem.at[0]).wait()

    @pl.when(parity == 0)
    def _():
        pltpu.make_async_copy(vb_hbm, basis.at[c, fs], load_sem.at[1]).wait()

    pltpu.make_async_copy(w_hbm, weights.at[fs], load_sem.at[8]).wait()
    pl.semaphore_wait(barrier, NZ - 1 + NY * NX * NC - 1)

    def offset(n, p):
        odd = lax.rem(n + p, 2)
        return (n + 1) * odd - n * (1 - odd)

    def from_z(n, p):
        return lax.rem(z - offset(n, p) + NZ, NZ)

    def bz(n):
        to = lax.rem(z + offset(n, parity) + NZ, NZ)
        return remote(shard, basis.at[c, fs], bz_s.at[n], bz_r.at[n], zdev(to))

    def bz_recv(n):
        block = basis.at[c, from_z(n, parity) * NY + y]
        return remote(block, block, bz_s.at[n], bz_r.at[n], zdev(zup(1)))

    def by(n, j):
        block = basis.at[c, from_z(n, parity) * NY + y]
        return remote(block, block, by_s.at[n, j - 1], by_r.at[n, j - 1], ydev(yup(j)))

    def by_recv(n, j):
        block = basis.at[c, from_z(n, parity) * NY + yup(NY - j)]
        return remote(block, block, by_s.at[n, j - 1], by_r.at[n, j - 1], ydev(yup(1)))

    half = NY // 2

    def bx(n, d):
        block = basis.at[c, pl.ds(from_z(n, parity) * NY + d * half, half)]
        return remote(block, block, bx_s.at[n, d], bx_r.at[n, d], xdev(xup(1 if d == 0 else NX - 1)))

    def bx_recv(n, d):
        block = basis.at[c, pl.ds(from_z(n, 1 - parity) * NY + d * half, half)]
        return remote(block, block, bx_s.at[n, d], bx_r.at[n, d], xdev(xup(1)))

    def bd(n, w):
        block = basis.at[c, pl.ds(from_z(n, parity if w == 0 else 1 - parity) * NY, NY)]
        return remote(block, block, bd_s.at[n, w], bd_r.at[n, w], sibling)

    def bd_recv(n, w):
        block = basis.at[1 - c, pl.ds(from_z(n, parity if w == 0 else 1 - parity) * NY, NY)]
        return remote(block, block, bd_s.at[n, w], bd_r.at[n, w], sibling)

    steps = NZ // 2

    def when_odd(n, act):
        if n == 0:
            pl.when(parity == 1)(act)
        else:
            act()

    for n in range(steps):
        when_odd(n, lambda n=n: bz(n).start())

    def wz(j):
        block = weights.at[fs]
        return remote(block, block, wz_s.at[j - 1], wz_r.at[j - 1], zdev(zup(j)))

    def wz_recv(j):
        block = weights.at[zup(NZ - j) * NY + y]
        return remote(block, block, wz_s.at[j - 1], wz_r.at[j - 1], zdev(zup(1)))

    def wy(i, j):
        block = weights.at[i * NY + y]
        return remote(block, block, wy_s.at[i, j - 1], wy_r.at[i, j - 1], ydev(yup(j)))

    def wy_recv(i, j):
        block = weights.at[i * NY + yup(NY - j)]
        return remote(block, block, wy_s.at[i, j - 1], wy_r.at[i, j - 1], ydev(yup(1)))

    for j in FAR_FIRST:
        wz(j).start()

    lag_y, lag_x = 2, 4
    for s in range(steps + lag_x):
        if s < steps:
            when_odd(s, lambda s=s: bz_recv(s).wait_recv())
            for j in range(1, NY):
                by(s, j).start()
        n = s - lag_y
        if 0 <= n < steps:
            for j in range(1, NY):
                by_recv(n, j).wait_recv()
            bx(n, 0).start()
            bx(n, 1).start()
            bd(n, 0).start()
        n = s - lag_x
        if 0 <= n < steps:
            bx_recv(n, 0).wait_recv()
            bx_recv(n, 1).wait_recv()
            bd(n, 1).start()

    for n in range(steps):
        for w in range(2):
            bd_recv(n, w).wait_recv()

    quarter = local // NY
    for k in range(2):
        whole = grads[k]
        high = whole.astype(jnp.bfloat16)
        low = (whole - high.astype(jnp.float32)).astype(jnp.bfloat16)
        base = basis[k].reshape(-1, rank)
        part = jnp.dot(high, base, preferred_element_type=jnp.float32) + jnp.dot(
            low, base, preferred_element_type=jnp.float32
        )
        ysend[k] = (part * scaling).reshape(NY, quarter, rank)
        for j in (2, 1, 3):
            remote(
                ysend.at[k, yup(j)], yrecv.at[k, j - 1], ry_s.at[k, j - 1], ry_r.at[k, j - 1], ydev(yup(j))
            ).start()

    for j in FAR_FIRST:
        wz_recv(j).wait_recv()
    for i in range(NZ):
        for j in range(1, NY):
            wy(i, j).start()

    def ry_recv(k, j):
        return remote(ysend.at[k, 0], yrecv.at[k, j - 1], ry_s.at[k, j - 1], ry_r.at[k, j - 1], ydev(yup(j)))

    piece = 2 * quarter // NZ
    for k in range(2):
        for j in range(1, NY):
            ry_recv(k, j).wait_recv()
        total = (ysend[k, y] + yrecv[k, 0]) + (yrecv[k, 1] + yrecv[k, 2])
        for i in range(NZ // 2):
            zsend[k * (NZ // 2) + i] = total[i * piece : (i + 1) * piece]

    def rz(j):
        return remote(zsend.at[zup(j)], zrecv.at[j - 1], rz_s.at[j - 1], rz_r.at[j - 1], zdev(zup(j)))

    for j in FAR_FIRST:
        rz(j).start()
    total = zsend[z]
    for j in reversed(FAR_FIRST):
        rz(j).wait_recv()
        total = total + zrecv[j - 1]
    lows[y, z] = total.astype(jnp.bfloat16)

    def az(j):
        block = lows.at[y, z]
        return remote(block, block, az_s.at[j - 1], az_r.at[j - 1], zdev(zup(j)))

    def az_recv(j):
        block = lows.at[y, zup(NZ - j)]
        return remote(block, block, az_s.at[j - 1], az_r.at[j - 1], zdev(zup(1)))

    for j in FAR_FIRST:
        az(j).start()
    for j in reversed(FAR_FIRST):
        az_recv(j).wait_recv()

    def ay(j):
        block = lows.at[y]
        return remote(block, block, ay_s.at[j - 1], ay_r.at[j - 1], ydev(yup(j)))

    def ay_recv(j):
        block = lows.at[yup(NY - j)]
        return remote(block, block, ay_s.at[j - 1], ay_r.at[j - 1], ydev(yup(1)))

    for j in (2, 1, 3):
        ay(j).start()

    mine = lows[y].astype(jnp.float32)
    square = jnp.sum(mine * mine)
    sums[here] = jnp.full((1, 128), square, jnp.float32)

    def cl(j):
        block = sums.at[here]
        return remote(block, block, cl_s.at[j - 1], cl_r.at[j - 1], plane(j))

    def cl_recv(j):
        block = sums.at[lax.rem(here + NY * NX * NC - j, NY * NX * NC)]
        return remote(block, block, cl_s.at[j - 1], cl_r.at[j - 1], plane(1))

    for j in range(1, NY * NX * NC):
        cl(j).start()
    for j in (1, 3, 2):
        ay_recv(j).wait_recv()
    for k in range(2):
        for yy in range(NY):
            for i in range(NZ // 2):
                at = yy * quarter + i * piece
                small[k, at : at + piece, :] = lows[yy, k * (NZ // 2) + i].astype(jnp.float32)
    for j in range(1, NY * NX * NC):
        cl_recv(j).wait_recv()
    everyone = jnp.sum(sums[...], axis=0)
    clip = 1.0 / jnp.sqrt(1.0 + everyone[:, 0:1] / entries)

    for i, (far, near) in enumerate(
        (
            (vmean_hbm, vstate.at[0]),
            (vsq_hbm, vstate.at[1]),
            (omean_hbm, ostate.at[0]),
            (osq_hbm, ostate.at[1]),
        )
    ):
        pltpu.make_async_copy(far, near, load_sem.at[4 + i]).wait()

    def advance(low, state, mean_out, sq_out):
        scaled = low * clip
        mean = 0.8 * state[0] + 0.2 * scaled
        sq = 0.9 * state[1] + 0.1 * scaled * scaled
        mean_out[...] = mean
        sq_out[...] = sq
        return mean / jnp.sqrt(sq + 0.1)

    norms = (
        advance(small[0].T, vstate, vmean_out, vsq_out),
        advance(small[1], ostate, omean_out, osq_out).T,
    )
    for i in range(NZ):
        for j in range(1, NY):
            wy_recv(i, j).wait_recv()
    copies = (vcopy_out, ocopy_out)
    block_rows = 256
    per = block_rows // rows
    for k in range(2):
        high = norms[k].astype(jnp.bfloat16)
        low = (norms[k] - high.astype(jnp.float32)).astype(jnp.bfloat16)
        both = jnp.concatenate([high, low], axis=1)
        for b in range(width // block_rows):
            base = basis[k, b * per : (b + 1) * per].reshape(block_rows, rank)
            step = jnp.dot(base, both, preferred_element_type=jnp.float32)
            step = step[:, :local] + step[:, local:]
            weight = decoded(weights[b * per : (b + 1) * per, k].reshape(block_rows, local))
            copies[k][b * block_rows : (b + 1) * block_rows, :] = (weight - 0.02 * step).astype(jnp.bfloat16)
        step = jnp.dot(basis[k, fs], both, preferred_element_type=jnp.float32)
        own_out[k] = step[:, :local] + step[:, local:]

    for i in range(NZ):
        for j in range(1, NY):
            wy(i, j).wait_send()
    for n in range(steps):
        when_odd(n, lambda n=n: bz(n).wait_send())
        for j in range(1, NY):
            by(n, j).wait_send()
        for w in range(2):
            bx(n, w).wait_send()
            bd(n, w).wait_send()
    for j in range(1, NZ):
        wz(j).wait_send()
        rz(j).wait_send()
        az(j).wait_send()
    for j in range(1, NY):
        ay(j).wait_send()
        for k in range(2):
            ry_recv(k, j).wait_send()
    for j in range(1, NY * NX * NC):
        cl(j).wait_send()


def on_device(
    block_input,
    value_cotangent,
    mixed_output,
    output_cotangent,
    value_weight,
    output_weight,
    value_basis,
    output_basis,
    value_mean,
    value_square,
    output_mean,
    output_square,
):
    tokens, width = block_input.shape
    local = value_cotangent.shape[1]
    rows, rank = value_basis.shape
    devices = lax.axis_size("fs")
    scaling = 1.0 / math.sqrt(tokens * devices)
    entries = 2.0 * rank * local * lax.axis_size("tp")
    quarter = local // NY
    piece = 2 * quarter // NZ
    f32, bf16 = jnp.float32, jnp.bfloat16
    sent = coded(jnp.stack([value_weight, output_weight.T]))
    hbm = pl.BlockSpec(memory_space=pl.ANY)
    vmem = pl.BlockSpec(memory_space=pltpu.VMEM)
    dma = pltpu.SemaphoreType.DMA
    near = NY * NX * NC - 1
    out = pl.pallas_call(
        functools.partial(kernel, scaling, entries),
        out_shape=(
            jax.ShapeDtypeStruct((rank, local), f32),
            jax.ShapeDtypeStruct((rank, local), f32),
            jax.ShapeDtypeStruct((local, rank), f32),
            jax.ShapeDtypeStruct((local, rank), f32),
            jax.ShapeDtypeStruct((width, local), bf16),
            jax.ShapeDtypeStruct((width, local), bf16),
            jax.ShapeDtypeStruct((2, rows, local), f32),
        ),
        in_specs=[hbm] * 11,
        out_specs=(vmem,) * 7,
        scratch_shapes=[
            pltpu.VMEM((tokens, width), bf16),
            pltpu.VMEM((tokens, width), bf16),
            pltpu.VMEM((tokens, local), bf16),
            pltpu.VMEM((tokens, local), bf16),
            pltpu.VMEM((rows, rank), bf16),
            pltpu.VMEM((2, devices, rows, rank), bf16),
            pltpu.VMEM((devices, 2, rows, local), bf16),
            pltpu.VMEM((2, local, width), f32),
            pltpu.VMEM((2, NY, quarter, rank), f32),
            pltpu.VMEM((2, NY - 1, quarter, rank), f32),
            pltpu.VMEM((NZ, piece, rank), f32),
            pltpu.VMEM((NZ - 1, piece, rank), f32),
            pltpu.VMEM((NY, NZ, piece, rank), bf16),
            pltpu.VMEM((NY * NX * NC, 1, 128), f32),
            pltpu.VMEM((2, local, rank), f32),
            pltpu.VMEM((2, rank, local), f32),
            pltpu.VMEM((2, local, rank), f32),
            dma((9,)),
            dma((2, CHUNKS)),
            dma((NZ // 2,)),
            dma((NZ // 2,)),
            dma((NZ // 2, NY - 1)),
            dma((NZ // 2, NY - 1)),
            dma((NZ // 2, 2)),
            dma((NZ // 2, 2)),
            dma((NZ // 2, 2)),
            dma((NZ // 2, 2)),
            dma((2, NY - 1)),
            dma((2, NY - 1)),
            dma((NZ - 1,)),
            dma((NZ - 1,)),
            dma((NZ - 1,)),
            dma((NZ - 1,)),
            dma((NY - 1,)),
            dma((NY - 1,)),
            dma((near,)),
            dma((near,)),
            dma((NZ - 1,)),
            dma((NZ - 1,)),
            dma((NZ, NY - 1)),
            dma((NZ, NY - 1)),
        ],
        compiler_params=pltpu.CompilerParams(
            collective_id=0, has_side_effects=True, vmem_limit_bytes=60 * 1024 * 1024
        ),
    )(
        block_input,
        value_cotangent,
        mixed_output,
        output_cotangent,
        value_basis,
        output_basis,
        sent,
        value_mean,
        value_square,
        output_mean,
        output_square,
    )
    value_mean_next, value_square_next, output_mean_next, output_square_next, value_copy, turned, own = out
    output_copy = turned.T
    value_step = own[0]
    output_step = own[1].T
    value_next = value_weight - 0.02 * value_step
    output_next = output_weight - 0.02 * output_step
    return (
        value_next,
        value_copy,
        value_step,
        value_mean_next,
        value_square_next,
        output_next,
        output_copy,
        output_step,
        output_mean_next,
        output_square_next,
    )


def solution(mesh):
    return jax.shard_map(
        on_device,
        mesh=mesh,
        in_specs=(
            P("fs", None),
            P("fs", "tp"),
            P("fs", "tp"),
            P("fs", None),
            P("fs", "tp"),
            P("tp", "fs"),
            P("fs", None),
            P("fs", None),
            P(None, "tp"),
            P(None, "tp"),
            P("tp", None),
            P("tp", None),
        ),
        out_specs=(
            P("fs", "tp"),
            P(None, "tp"),
            P("fs", "tp"),
            P(None, "tp"),
            P(None, "tp"),
            P("tp", "fs"),
            P("tp", None),
            P("tp", "fs"),
            P("tp", None),
            P("tp", None),
        ),
        check_vma=False,
    )
```

time: 507 us -> 93.5 us (0.18)
  waiting for transfers between devices: 430 us -> 0 us
  Pallas kernels: 0 us -> 77.9 us
  blocking collectives: 19.3 us -> 0 us
  starting transfers between devices: 15.3 us -> 0 us
  between operations: 15.4 us -> 0.66 us
  matrix products: 7.61 us -> 0 us
    psum x1 -> x0, waiting for transfers between devices: 268 us -> none  [together(): so_far = lax.psum(flat, axis)]
    reduce_scatter x2 -> x0, waiting for transfers between devices: 104 us -> none  [own_block(): parts = lax.psum_scatter(parts, axes[k], scatter_dimension=0, tiled=True)]
    pallas_call x0 -> x1, Pallas kernels: none -> 77.9 us  [on_device(): pl.pallas_call(functools.partial(kernel, scaling, entries), out_shape=(ja...]
    all_to_all x2 -> x0, waiting for transfers between devices: 58.3 us -> none  [from_everyone(): return lax.all_to_all(copies, axis, split_axis=0, concat_axis=0, tiled=True)]
    all_to_all x1 -> x0, blocking collectives: 19.3 us -> none  [from_everyone(): return lax.all_to_all(copies, axis, split_axis=0, concat_axis=0, tiled=True)]
    all_to_all x2 -> x0, starting transfers between devices: 15.2 us -> none  [from_everyone(): return lax.all_to_all(copies, axis, split_axis=0, concat_axis=0, tiled=True)]
    dot_general x6 -> x0, matrix products: 7.61 us -> none  [the longest x1 3.09 us: on_device(): lax.dot_general(block_input, value_cotangent, contract, preferred_element...]
    unnamed x34 -> x10, local copies, waits for them, and re-layouts: 3.12 us -> 10.4 us
  transfers between devices with their start and end apart: 5 -> 0, of which waited for: 5 -> 0; matrix products, arithmetic and copies ran while one was open for 0% -> 0% of each run, Pallas kernels for 0% -> 0%
where the time goes in v1:
time: 93.5 us; the launch traced here: 93 us
  Pallas kernels  77.9 us (83%)
  local copies, waits for them, and re-layouts  10.4 us (11%)
  other arithmetic  4.02 us (4%)
    pallas_call x1, Pallas kernels, on_device(): pl.pallas_call(functools.partial(kernel, scaling, entries), out_shape=(ja...  77.9 us
    unnamed x10, local copies, waits for them, and re-layouts  10.4 us

profile of v1, /device:TPU:1, one launch (start us, length us, event | category | flops | bytes accessed | tf_op | source)
XLA Modules:
  0.0 93.0 jit_solution(1205776105817339327)
XLA Ops:
  0.6 1.4 %fusion.w_hbm = bf16[2,32,128]{2,1,0:T(8,128)(2,1)} fusion(f32[1,32,128]{2,1,0:T(8,128)} %bitcast.14, f32[1,32,128]{2,1,0:T(8,128)} %bitcast.15), kind=kLoop, calls=%fused_computation.1 | loop fusion | flops 73728 | bytes 49152 | tf_op jit(solution)/shard_map/convert_element_type | solution.py:21
  2.0 0.0 copy-start
  2.0 0.0 copy-start.1
  2.0 77.9 %shard_map.195 = (f32[384,128]{1,0:T(8,128)}, f32[384,128]{1,0:T(8,128)}, f32[128,384]{1,0:T(8,128)}, f32[128,384]{1,0:T(8,128)}, bf16[2048,128]{1,0:T(8,128)(2,...) custom-call(bf16[1024,2048]{1,0:T(8,128)(2,1)} %x_hbm.1, bf16[1024,128]{1,0:T(8,128)(2,1)} %v_hbm.1, ...), custom_call_target="tpu_custom_call" | custom-call | tf_op jit(solution)/shard_map/pallas_call | solution.py:462
  79.9 0.0 copy-done
  80.0 1.3 %multiply_subtract_fusion = (f32[128,32]{0,1:T(8,128)}, f32[128,32]{0,1:T(8,128)}) fusion(f32[128,32]{0,1:T(8,128)S(1)} %copy-done, f32[2,32,128]{2,1,0:T(8,128)} %get-tuple-element.17), kind=kLoop, calls=%fused_computation.3 | loop fusion | flops 8192 | bytes 65536 | tf_op jit(solution)/shard_map/sub | solution.py:539
  81.3 0.0 copy-done.1
  81.3 1.3 %multiply_subtract_fusion.1 = (f32[32,128]{1,0:T(8,128)}, f32[32,128]{1,0:T(8,128)}) fusion(f32[32,128]{1,0:T(8,128)S(1)} %copy-done.1, f32[2,32,128]{2,1,0:T(8,128)} %get-tuple-element.17), kind=kLoop, calls=%fused_computation.5 | loop fusion | flops 8192 | bytes 65536 | tf_op jit(solution)/shard_map/sub | solution.py:538
  82.6 2.0 %copy.22 = bf16[128,2048]{1,0:T(8,128)(2,1)} copy(bf16[128,2048]{0,1:T(8,128)(2,1)} %bitcast.13) | data formatting | bytes 1048576
  84.7 1.9 %copy.28 = bf16[2048,128]{1,0:T(8,128)(2,1)} copy(bf16[2048,128]{1,0:T(8,128)(2,1)} %get-tuple-element.49) | data formatting | bytes 1048576
  86.5 1.6 %copy.29 = f32[384,128]{1,0:T(8,128)} copy(f32[384,128]{1,0:T(8,128)} %get-tuple-element.51) | data formatting | bytes 393216
  88.2 1.6 %copy.30 = f32[384,128]{1,0:T(8,128)} copy(f32[384,128]{1,0:T(8,128)} %get-tuple-element.52) | data formatting | bytes 393216
  89.8 1.6 %copy.31 = f32[128,384]{1,0:T(8,128)} copy(f32[128,384]{1,0:T(8,128)} %get-tuple-element.56) | data formatting | bytes 393216
  91.4 1.6 %copy.32 = f32[128,384]{1,0:T(8,128)} copy(f32[128,384]{1,0:T(8,128)} %get-tuple-element.57) | data formatting | bytes 393216
Async XLA Ops:
  2.0 77.9 %copy-start = (f32[128,32]{0,1:T(8,128)S(1)}, f32[128,32]{0,1:T(8,128)}, u32[]{:S(2)}) copy-start(f32[128,32]{0,1:T(8,128)} %param.17) | copy-start | bytes 49156
  2.0 79.3 %copy-start.1 = (f32[32,128]{1,0:T(8,128)S(1)}, f32[32,128]{1,0:T(8,128)}, u32[]{:S(2)}) copy-start(f32[32,128]{1,0:T(8,128)} %param.16) | copy-start | bytes 49156

commit v2 on v1

v2 whole, which is shorter than its diff:
```python
import functools
import math

import jax
import jax.numpy as jnp
from jax import lax
from jax.experimental import pallas as pl
from jax.experimental.pallas import tpu as pltpu
from jax.sharding import PartitionSpec as P

NZ, NY, NX, NC = 16, 4, 4, 2
MESH = pl.DeviceIdType.MESH
W_BOUND = 0.1875
W_SLOPE = 250.0 / W_BOUND
CHUNKS = 4
NEAR = (4, 12, 3, 13, 2, 14, 1, 15)
IN_ORDER = (0, 1, 15, 2, 14, 3, 13, 4, 12, 5, 11, 6, 10, 7, 9, 8)
RELAYED = {4: (4, 3, 2, 1), 12: (-3, -2, -1)}
LAG_Y, LAG_X = 5, 9
FAR_FIRST = (8, 7, 9, 6, 10, 5, 11, 4, 12, 3, 13, 2, 14, 1, 15)


def coded(weight):
    size = jnp.exp2(jnp.abs(weight) * W_SLOPE - 125.0)
    return jnp.where(weight < 0, -size, size).astype(jnp.bfloat16)


def decoded(code):
    code = code.astype(jnp.float32)
    size = (jnp.log2(jnp.abs(code)) + 125.0) * (1.0 / W_SLOPE)
    return jnp.where(code < 0, -size, size)


def kernel(
    scaling,
    entries,
    x_hbm,
    v_hbm,
    m_hbm,
    oc_hbm,
    vb_hbm,
    ob_hbm,
    vw_hbm,
    ow_hbm,
    vmean_hbm,
    vsq_hbm,
    omean_hbm,
    osq_hbm,
    vnext_out,
    vcopy_out,
    vstep_out,
    vmean_out,
    vsq_out,
    onext_out,
    ocopy_out,
    ostep_out,
    omean_out,
    osq_out,
    xs,
    ocs,
    vs,
    ms,
    basis,
    owned,
    weights,
    grads,
    ysend,
    yrecv,
    zsend,
    zrecv,
    lows,
    sums,
    small,
    vstate,
    ostate,
    load_sem,
    chunk_sem,
    bz_s,
    bz_r,
    by_s,
    by_r,
    bx_s,
    bx_r,
    bd_s,
    bd_r,
    ry_s,
    ry_r,
    rz_s,
    rz_r,
    az_s,
    az_r,
    ay_s,
    ay_r,
    cl_s,
    cl_r,
    wz_s,
    wz_r,
    wy_s,
    wy_r,
):
    fs, tp = lax.axis_index("fs"), lax.axis_index("tp")
    z, y = fs // NY, lax.rem(fs, NY)
    x, c = tp // NC, lax.rem(tp, NC)
    parity = lax.rem(x, 2)
    tokens, width = xs.shape
    rank = basis.shape[3]
    local = vs.shape[1]
    rows = basis.shape[2]

    def zdev(zz):
        return {"fs": zz * NY + y, "tp": tp}

    def ydev(yy):
        return {"fs": z * NY + yy, "tp": tp}

    def xdev(xx):
        return {"fs": fs, "tp": xx * NC + c}

    sibling = {"fs": fs, "tp": x * NC + 1 - c}

    def zup(j):
        return lax.rem(z + j, NZ)

    def yup(j):
        return lax.rem(y + j, NY)

    def xup(j):
        return lax.rem(x + j, NX)

    pending = []

    def go(copy):
        copy.start()
        pending.append(copy)

    def remote(src, dst, ssem, rsem, device):
        return pltpu.make_async_remote_copy(
            src_ref=src, dst_ref=dst, send_sem=ssem, recv_sem=rsem, device_id=device, device_id_type=MESH
        )

    here = y * (NX * NC) + tp

    def plane(j):
        other = lax.rem(here + j, NY * NX * NC)
        return {"fs": z * NY + other // (NX * NC), "tp": lax.rem(other, NX * NC)}

    half = rows // 2

    def part_of(p):
        return pl.ds(pl.multiple_of(p * half, half), half)

    for k, far in enumerate((vb_hbm, ob_hbm)):

        @pl.when(c == k)
        def _(k=k, far=far):
            pltpu.make_async_copy(far.at[part_of(parity)], basis.at[k, fs, part_of(parity)], load_sem.at[0]).start()

    pltpu.make_async_copy(vw_hbm, owned.at[0], load_sem.at[1]).start()
    pltpu.make_async_copy(ow_hbm, owned.at[1], load_sem.at[8]).start()
    pltpu.make_async_copy(v_hbm, vs, load_sem.at[2]).start()
    pltpu.make_async_copy(m_hbm, ms, load_sem.at[3]).start()
    size = tokens // CHUNKS
    for t in range(CHUNKS):
        at = pl.ds(t * size, size)
        pltpu.make_async_copy(x_hbm.at[at], xs.at[at], chunk_sem.at[0, t]).start()
        pltpu.make_async_copy(oc_hbm.at[at], ocs.at[at], chunk_sem.at[1, t]).start()
    pltpu.make_async_copy(vmean_hbm, vstate.at[0], load_sem.at[4]).start()
    pltpu.make_async_copy(vsq_hbm, vstate.at[1], load_sem.at[5]).start()
    pltpu.make_async_copy(omean_hbm, ostate.at[0], load_sem.at[6]).start()
    pltpu.make_async_copy(osq_hbm, ostate.at[1], load_sem.at[7]).start()

    barrier = pltpu.get_barrier_semaphore()
    for j in NEAR:
        pl.semaphore_signal(barrier, inc=1, device_id=zdev(zup(j)), device_id_type=MESH)
    for j in range(1, NY * NX * NC):
        pl.semaphore_signal(barrier, inc=1, device_id=plane(j), device_id_type=MESH)

    pltpu.make_async_copy(vb_hbm.at[part_of(0)], basis.at[c, fs, part_of(parity)], load_sem.at[0]).wait()
    pltpu.make_async_copy(vw_hbm, owned.at[0], load_sem.at[1]).wait()
    pltpu.make_async_copy(ow_hbm, owned.at[1], load_sem.at[8]).wait()
    weights[fs] = coded(owned[...])

    pltpu.make_async_copy(v_hbm, vs, load_sem.at[2]).wait()
    pltpu.make_async_copy(m_hbm, ms, load_sem.at[3]).wait()
    across = (((0,), (0,)), ((), ()))
    for t in range(CHUNKS):
        at = pl.ds(t * size, size)
        for k, (far, near, thin) in enumerate(((x_hbm, xs, vs), (oc_hbm, ocs, ms))):
            pltpu.make_async_copy(far.at[at], near.at[at], chunk_sem.at[k, t]).wait()
            part = lax.dot_general(thin[at, :], near[at, :], across, preferred_element_type=jnp.float32)
            if t == 0:
                grads[k] = part
            else:
                grads[k] += part

    pl.semaphore_wait(barrier, len(NEAR) + NY * NX * NC - 1)

    def relay(block_of, ssem, rsem):
        def down(d, to):
            block = block_of(zup(NZ - d if d else 0))
            at = (d + to) % NZ - 1
            return remote(block, block, ssem.at[at], rsem.at[at], zdev(zup(to % NZ)))

        def arrived(d):
            block = block_of(zup(NZ - d))
            remote(block, block, ssem.at[d - 1], rsem.at[d - 1], zdev(zup(1))).wait_recv()

        return down, arrived

    def basis_row(zz):
        return basis.at[c, zz * NY + y, part_of(parity)]

    def weight_row(zz):
        return weights.at[zz * NY + y]

    send_basis, basis_came = relay(basis_row, bz_s, bz_r)
    send_weight, weight_came = relay(weight_row, wz_s, wz_r)

    def by(d, j):
        block = basis_row(zup(NZ - d if d else 0))
        return remote(block, block, by_s.at[d, j - 1], by_r.at[d, j - 1], ydev(yup(j)))

    def by_recv(d, j):
        block = basis.at[c, zup(NZ - d if d else 0) * NY + yup(NY - j), part_of(parity)]
        return remote(block, block, by_s.at[d, j - 1], by_r.at[d, j - 1], ydev(yup(1)))

    pair = NY // 2

    def bx(d, w):
        block = basis.at[c, pl.ds(zup(NZ - d if d else 0) * NY + w * pair, pair), part_of(parity)]
        return remote(block, block, bx_s.at[d, w], bx_r.at[d, w], xdev(xup(1 if w == 0 else NX - 1)))

    def bx_recv(d, w):
        block = basis.at[c, pl.ds(zup(NZ - d if d else 0) * NY + w * pair, pair), part_of(1 - parity)]
        return remote(block, block, bx_s.at[d, w], bx_r.at[d, w], xdev(xup(1)))

    def bd(d, w):
        block = basis.at[c, pl.ds(zup(NZ - d if d else 0) * NY, NY), part_of(parity if w == 0 else 1 - parity)]
        return remote(block, block, bd_s.at[d, w], bd_r.at[d, w], sibling)

    def bd_recv(d, w):
        block = basis.at[1 - c, pl.ds(zup(NZ - d if d else 0) * NY, NY), part_of(parity if w == 0 else 1 - parity)]
        return remote(block, block, bd_s.at[d, w], bd_r.at[d, w], sibling)

    for to in NEAR:
        go(send_basis(0, to))
    for s in range(NZ + LAG_X):
        if s < NZ:
            d = IN_ORDER[s]
            if d:
                basis_came(d)
            if d in RELAYED:
                for to in RELAYED[d]:
                    go(send_basis(d, to))
            for j in (2, 1, 3):
                go(by(d, j))
        if 0 <= s - LAG_Y < NZ:
            d = IN_ORDER[s - LAG_Y]
            for j in range(1, NY):
                by_recv(d, j).wait_recv()
            for w in range(2):
                go(bx(d, w))
            go(bd(d, 0))
        if s == NZ:
            for to in NEAR:
                go(send_weight(0, to))
        if 0 <= s - LAG_X < NZ:
            d = IN_ORDER[s - LAG_X]
            for w in range(2):
                bx_recv(d, w).wait_recv()
            go(bd(d, 1))

    def wy(d, j):
        block = weight_row(zup(NZ - d if d else 0))
        return remote(block, block, wy_s.at[d, j - 1], wy_r.at[d, j - 1], ydev(yup(j)))

    def wy_recv(d, j):
        block = weights.at[zup(NZ - d if d else 0) * NY + yup(NY - j)]
        return remote(block, block, wy_s.at[d, j - 1], wy_r.at[d, j - 1], ydev(yup(1)))

    for d in IN_ORDER:
        for w in range(2):
            bd_recv(d, w).wait_recv()

    quarter = local // NY
    for k in range(2):
        whole = grads[k]
        high = whole.astype(jnp.bfloat16)
        low = (whole - high.astype(jnp.float32)).astype(jnp.bfloat16)
        base = basis[k].reshape(-1, rank)
        part = jnp.dot(high, base, preferred_element_type=jnp.float32) + jnp.dot(
            low, base, preferred_element_type=jnp.float32
        )
        ysend[k] = (part * scaling).reshape(NY, quarter, rank)
        for j in (2, 1, 3):
            go(
                remote(
                    ysend.at[k, yup(j)], yrecv.at[k, j - 1], ry_s.at[k, j - 1], ry_r.at[k, j - 1], ydev(yup(j))
                )
            )

    for d in IN_ORDER[1:9]:
        weight_came(d)
        for to in RELAYED.get(d, ()):
            go(send_weight(d, to))

    def ry_recv(k, j):
        return remote(ysend.at[k, 0], yrecv.at[k, j - 1], ry_s.at[k, j - 1], ry_r.at[k, j - 1], ydev(yup(j)))

    piece = 2 * quarter // NZ
    for k in range(2):
        for j in range(1, NY):
            ry_recv(k, j).wait_recv()
        total = (ysend[k, y] + yrecv[k, 0]) + (yrecv[k, 1] + yrecv[k, 2])
        for i in range(NZ // 2):
            zsend[k * (NZ // 2) + i] = total[i * piece : (i + 1) * piece]

    def rz(j):
        return remote(zsend.at[zup(j)], zrecv.at[j - 1], rz_s.at[j - 1], rz_r.at[j - 1], zdev(zup(j)))

    for j in FAR_FIRST:
        go(rz(j))
    for d in IN_ORDER[:9]:
        for j in (2, 1, 3):
            go(wy(d, j))
    total = zsend[z]
    for j in reversed(FAR_FIRST):
        rz(j).wait_recv()
        total = total + zrecv[j - 1]
    lows[y, z] = total.astype(jnp.bfloat16)

    def az(j):
        block = lows.at[y, z]
        return remote(block, block, az_s.at[j - 1], az_r.at[j - 1], zdev(zup(j)))

    def az_recv(j):
        block = lows.at[y, zup(NZ - j)]
        return remote(block, block, az_s.at[j - 1], az_r.at[j - 1], zdev(zup(1)))

    for j in FAR_FIRST:
        go(az(j))
    for d in IN_ORDER[9:]:
        weight_came(d)
        for j in (2, 1, 3):
            go(wy(d, j))
    for j in reversed(FAR_FIRST):
        az_recv(j).wait_recv()

    def ay(j):
        block = lows.at[y]
        return remote(block, block, ay_s.at[j - 1], ay_r.at[j - 1], ydev(yup(j)))

    def ay_recv(j):
        block = lows.at[yup(NY - j)]
        return remote(block, block, ay_s.at[j - 1], ay_r.at[j - 1], ydev(yup(1)))

    for j in (2, 1, 3):
        go(ay(j))

    mine = lows[y].astype(jnp.float32)
    square = jnp.sum(mine * mine)
    sums[here] = jnp.full((1, 128), square, jnp.float32)

    def cl(j):
        block = sums.at[here]
        return remote(block, block, cl_s.at[j - 1], cl_r.at[j - 1], plane(j))

    def cl_recv(j):
        block = sums.at[lax.rem(here + NY * NX * NC - j, NY * NX * NC)]
        return remote(block, block, cl_s.at[j - 1], cl_r.at[j - 1], plane(1))

    for j in range(1, NY * NX * NC):
        go(cl(j))
    for j in (1, 3, 2):
        ay_recv(j).wait_recv()
    for k in range(2):
        for yy in range(NY):
            for i in range(NZ // 2):
                at = yy * quarter + i * piece
                small[k, at : at + piece, :] = lows[yy, k * (NZ // 2) + i].astype(jnp.float32)
    for j in range(1, NY * NX * NC):
        cl_recv(j).wait_recv()
    everyone = jnp.sum(sums[...], axis=0)
    clip = 1.0 / jnp.sqrt(1.0 + everyone[:, 0:1] / entries)

    for i, (far, near) in enumerate(
        (
            (vmean_hbm, vstate.at[0]),
            (vsq_hbm, vstate.at[1]),
            (omean_hbm, ostate.at[0]),
            (osq_hbm, ostate.at[1]),
        )
    ):
        pltpu.make_async_copy(far, near, load_sem.at[4 + i]).wait()

    def advance(low, state, mean_out, sq_out):
        scaled = low * clip
        mean = 0.8 * state[0] + 0.2 * scaled
        sq = 0.9 * state[1] + 0.1 * scaled * scaled
        mean_out[...] = mean
        sq_out[...] = sq
        return mean / jnp.sqrt(sq + 0.1)

    norms = (
        advance(small[0].T, vstate, vmean_out, vsq_out),
        advance(small[1], ostate, omean_out, osq_out).T,
    )
    for d in IN_ORDER:
        for j in range(1, NY):
            wy_recv(d, j).wait_recv()
    block_rows = 256
    per = block_rows // rows
    for k in range(2):
        high = norms[k].astype(jnp.bfloat16)
        low = (norms[k] - high.astype(jnp.float32)).astype(jnp.bfloat16)
        both = jnp.concatenate([high, low], axis=1)
        for b in range(width // block_rows):
            base = basis[k, b * per : (b + 1) * per].reshape(block_rows, rank)
            step = jnp.dot(base, both, preferred_element_type=jnp.float32)
            step = step[:, :local] + step[:, local:]
            weight = decoded(weights[b * per : (b + 1) * per, k].reshape(block_rows, local))
            moved = weight - 0.02 * step
            at = slice(b * block_rows, (b + 1) * block_rows)
            if k == 0:
                vcopy_out[at, :] = moved.astype(jnp.bfloat16)
            else:
                ocopy_out[:, at] = moved.T.astype(jnp.bfloat16)
        step = jnp.dot(basis[k, fs], both, preferred_element_type=jnp.float32)
        step = step[:, :local] + step[:, local:]
        (vstep_out, ostep_out)[k][...] = step
        (vnext_out, onext_out)[k][...] = owned[k] - 0.02 * step

    for copy in pending:
        copy.wait_send()


def store(*refs):
    count = len(refs) // 2
    for near, far in zip(refs[:count], refs[count:]):
        far[...] = near[...]


def on_device(
    block_input,
    value_cotangent,
    mixed_output,
    output_cotangent,
    value_weight,
    output_weight,
    value_basis,
    output_basis,
    value_mean,
    value_square,
    output_mean,
    output_square,
):
    tokens, width = block_input.shape
    local = value_cotangent.shape[1]
    rows, rank = value_basis.shape
    devices = lax.axis_size("fs")
    scaling = 1.0 / math.sqrt(tokens * devices)
    entries = 2.0 * rank * local * lax.axis_size("tp")
    quarter = local // NY
    piece = 2 * quarter // NZ
    f32, bf16 = jnp.float32, jnp.bfloat16
    hbm = pl.BlockSpec(memory_space=pltpu.HBM)
    vmem = pl.BlockSpec(memory_space=pltpu.VMEM)
    dma = pltpu.SemaphoreType.DMA
    near = NY * NX * NC - 1
    shapes = (
        jax.ShapeDtypeStruct((rows, local), f32),
        jax.ShapeDtypeStruct((width, local), bf16),
        jax.ShapeDtypeStruct((rows, local), f32),
        jax.ShapeDtypeStruct((rank, local), f32),
        jax.ShapeDtypeStruct((rank, local), f32),
        jax.ShapeDtypeStruct((rows, local), f32),
        jax.ShapeDtypeStruct((local, width), bf16),
        jax.ShapeDtypeStruct((rows, local), f32),
        jax.ShapeDtypeStruct((local, rank), f32),
        jax.ShapeDtypeStruct((local, rank), f32),
    )
    out = pl.pallas_call(
        functools.partial(kernel, scaling, entries),
        out_shape=shapes,
        in_specs=[hbm] * 12,
        out_specs=(vmem,) * len(shapes),
        scratch_shapes=[
            pltpu.VMEM((tokens, width), bf16),
            pltpu.VMEM((tokens, width), bf16),
            pltpu.VMEM((tokens, local), bf16),
            pltpu.VMEM((tokens, local), bf16),
            pltpu.VMEM((2, devices, rows, rank), bf16),
            pltpu.VMEM((2, rows, local), f32),
            pltpu.VMEM((devices, 2, rows, local), bf16),
            pltpu.VMEM((2, local, width), f32),
            pltpu.VMEM((2, NY, quarter, rank), f32),
            pltpu.VMEM((2, NY - 1, quarter, rank), f32),
            pltpu.VMEM((NZ, piece, rank), f32),
            pltpu.VMEM((NZ - 1, piece, rank), f32),
            pltpu.VMEM((NY, NZ, piece, rank), bf16),
            pltpu.VMEM((NY * NX * NC, 1, 128), f32),
            pltpu.VMEM((2, local, rank), f32),
            pltpu.VMEM((2, rank, local), f32),
            pltpu.VMEM((2, local, rank), f32),
            dma((9,)),
            dma((2, CHUNKS)),
            *[dma((NZ - 1,))] * 2,
            *[dma((NZ, NY - 1))] * 2,
            *[dma((NZ, 2))] * 4,
            *[dma((2, NY - 1))] * 2,
            *[dma((NZ - 1,))] * 4,
            *[dma((NY - 1,))] * 2,
            *[dma((near,))] * 2,
            *[dma((NZ - 1,))] * 2,
            *[dma((NZ, NY - 1))] * 2,
        ],
        compiler_params=pltpu.CompilerParams(
            collective_id=0, has_side_effects=True, vmem_limit_bytes=32 * 1024 * 1024
        ),
    )(
        block_input,
        value_cotangent,
        mixed_output,
        output_cotangent,
        value_basis,
        output_basis,
        value_weight,
        output_weight.T,
        value_mean,
        value_square,
        output_mean,
        output_square,
    )
    out = pl.pallas_call(
        store,
        out_shape=shapes,
        in_specs=[vmem] * len(shapes),
        out_specs=(vmem,) * len(shapes),
        compiler_params=pltpu.CompilerParams(vmem_limit_bytes=16 * 1024 * 1024),
    )(*out)
    out = list(out)
    out[5], out[7] = out[5].T, out[7].T
    return tuple(out)


def solution(mesh):
    return jax.shard_map(
        on_device,
        mesh=mesh,
        in_specs=(
            P("fs", None),
            P("fs", "tp"),
            P("fs", "tp"),
            P("fs", None),
            P("fs", "tp"),
            P("tp", "fs"),
            P("fs", None),
            P("fs", None),
            P(None, "tp"),
            P(None, "tp"),
            P("tp", None),
            P("tp", None),
        ),
        out_specs=(
            P("fs", "tp"),
            P(None, "tp"),
            P("fs", "tp"),
            P(None, "tp"),
            P(None, "tp"),
            P("tp", "fs"),
            P("tp", None),
            P("tp", "fs"),
            P("tp", None),
            P("tp", None),
        ),
        check_vma=False,
    )
```

time: 93.5 us -> 90 us (0.963)
  other arithmetic: 4.02 us -> 0 us
  local copies, waits for them, and re-layouts: 10.4 us -> 12.9 us
  Pallas kernels: 77.9 us -> 75.8 us
    sub x2 -> x0, other arithmetic: 2.66 us -> none  [the longest x1 1.33 us: on_device(): output_next = output_weight - 0.02 * output_step]
    unnamed x10 -> x24, local copies, waits for them, and re-layouts: 10.4 us -> 12.9 us
    pallas_call x1 -> x2, Pallas kernels: 77.9 us -> 75.8 us  [the longest x1 74.4 us: on_device(): pl.pallas_call(functools.partial(kernel, scaling, entries), out_shape=sha...]
    convert_element_type x1 -> x0, other arithmetic: 1.36 us -> none  [coded(): return jnp.where(weight < 0, -size, size).astype(jnp.bfloat16)]
where the time goes in v2:
time: 90 us; the launch traced here: 89.4 us
  Pallas kernels  75.8 us (84%)
  local copies, waits for them, and re-layouts  12.9 us (14%)
    pallas_call x1, Pallas kernels, on_device(): pl.pallas_call(functools.partial(kernel, scaling, entries), out_shape=sha...  74.4 us
    unnamed x24, local copies, waits for them, and re-layouts  12.9 us

profile of v2, /device:TPU:1, one launch (start us, length us, event | category | flops | bytes accessed | tf_op | source)
XLA Modules:
  0.0 89.4 jit_solution(5655503173793280864)
XLA Ops:
  0.6 0.0 copy-start
  0.7 2.2 %copy-done = bf16[1024,2048]{1,0:T(8,128)(2,1)S(1)} copy-done((bf16[1024,2048]{1,0:T(8,128)(2,1)S(1)}, bf16[1024,2048]{1,0:T(8,128)(2,1)}, u32[]{:S(2)}) %copy-start) | copy-done | bytes 4194328
  2.8 0.0 copy-start.1
  2.8 2.2 %copy-done.1 = bf16[1024,2048]{1,0:T(8,128)(2,1)S(1)} copy-done((bf16[1024,2048]{1,0:T(8,128)(2,1)S(1)}, bf16[1024,2048]{1,0:T(8,128)(2,1)}, u32[]{:S(2)}) %copy-start.1) | copy-done | bytes 4194328
  5.0 0.0 copy-start.2
  5.0 0.9 %copy-done.2 = bf16[1024,128]{1,0:T(8,128)(2,1)S(1)} copy-done((bf16[1024,128]{1,0:T(8,128)(2,1)S(1)}, bf16[1024,128]{1,0:T(8,128)(2,1)}, u32[]{:S(2)}) %copy-start.2) | copy-done | bytes 262168
  6.0 0.0 copy-start.3
  6.0 0.9 %copy-done.3 = bf16[1024,128]{1,0:T(8,128)(2,1)S(1)} copy-done((bf16[1024,128]{1,0:T(8,128)(2,1)S(1)}, bf16[1024,128]{1,0:T(8,128)(2,1)}, u32[]{:S(2)}) %copy-start.3) | copy-done | bytes 262168
  6.9 0.0 copy-start.4
  6.9 0.9 %copy-done.4 = f32[384,128]{1,0:T(8,128)S(1)} copy-done((f32[384,128]{1,0:T(8,128)S(1)}, f32[384,128]{1,0:T(8,128)}, u32[]{:S(2)}) %copy-start.4) | copy-done | bytes 196632
  7.9 0.0 copy-start.5
  7.9 0.9 %copy-done.5 = f32[384,128]{1,0:T(8,128)S(1)} copy-done((f32[384,128]{1,0:T(8,128)S(1)}, f32[384,128]{1,0:T(8,128)}, u32[]{:S(2)}) %copy-start.5) | copy-done | bytes 196632
  8.8 0.0 copy-start.6
  8.8 0.9 %copy-done.6 = f32[128,384]{1,0:T(8,128)S(1)} copy-done((f32[128,384]{1,0:T(8,128)S(1)}, f32[128,384]{1,0:T(8,128)}, u32[]{:S(2)}) %copy-start.6) | copy-done | bytes 196632
  9.7 0.0 copy-start.7
  9.7 0.9 %copy-done.7 = f32[128,384]{1,0:T(8,128)S(1)} copy-done((f32[128,384]{1,0:T(8,128)S(1)}, f32[128,384]{1,0:T(8,128)}, u32[]{:S(2)}) %copy-start.7) | copy-done | bytes 196632
  10.6 0.0 copy-start.8
  10.6 0.7 copy-done.8
  11.4 0.0 copy-start.9
  11.4 0.7 copy-done.9
  12.1 0.0 copy-start.10
  12.1 0.7 copy-done.10
  12.8 0.0 copy-start.11
  12.8 0.7 copy-done.11
  13.5 74.4 %shard_map.195 = (f32[32,128]{1,0:T(8,128)S(1)}, bf16[2048,128]{1,0:T(8,128)(2,1)S(1)}, f32[32,128]{1,0:T(8,128)S(1)}, f32[384,128]{1,0:T(8,128)S(1)}, f32[384,1...) custom-call(bf16[1024,2048]{1,0:T(8,128)(2,1)S(1)} %copy-done, ...), custom_call_target="tpu_custom_call" | custom-call | tf_op jit(solution)/shard_map/pallas_call | solution.py:482
  88.0 1.4 %shard_map.196 = (f32[32,128]{1,0:T(8,128)}, bf16[2048,128]{1,0:T(8,128)(2,1)}, f32[32,128]{1,0:T(8,128)}, f32[384,128]{1,0:T(8,128)}, f32[384,128]{1,0:T(8,128)...) custom-call(f32[32,128]{1,0:T(8,128)S(1)} %get-tuple-element.30.refs, ...), custom_call_target="tpu_custom_call" | custom-call | tf_op jit(solution)/shard_map/pallas_call | solution.py:534
Async XLA Ops:
  0.6 2.2 %copy-start = (bf16[1024,2048]{1,0:T(8,128)(2,1)S(1)}, bf16[1024,2048]{1,0:T(8,128)(2,1)}, u32[]{:S(2)}) copy-start(bf16[1024,2048]{1,0:T(8,128)(2,1)} %x_hbm.1) | copy-start | bytes 12582916
  2.8 2.2 %copy-start.1 = (bf16[1024,2048]{1,0:T(8,128)(2,1)S(1)}, bf16[1024,2048]{1,0:T(8,128)(2,1)}, u32[]{:S(2)}) copy-start(bf16[1024,2048]{1,0:T(8,128)(2,1)} %oc_hbm.1) | copy-start | bytes 12582916
  5.0 0.9 %copy-start.2 = (bf16[1024,128]{1,0:T(8,128)(2,1)S(1)}, bf16[1024,128]{1,0:T(8,128)(2,1)}, u32[]{:S(2)}) copy-start(bf16[1024,128]{1,0:T(8,128)(2,1)} %v_hbm.1) | copy-start | bytes 786436
  6.0 0.9 %copy-start.3 = (bf16[1024,128]{1,0:T(8,128)(2,1)S(1)}, bf16[1024,128]{1,0:T(8,128)(2,1)}, u32[]{:S(2)}) copy-start(bf16[1024,128]{1,0:T(8,128)(2,1)} %m_hbm.1) | copy-start | bytes 786436
  6.9 0.9 %copy-start.4 = (f32[384,128]{1,0:T(8,128)S(1)}, f32[384,128]{1,0:T(8,128)}, u32[]{:S(2)}) copy-start(f32[384,128]{1,0:T(8,128)} %vmean_hbm.1) | copy-start | bytes 589828
  7.9 0.9 %copy-start.5 = (f32[384,128]{1,0:T(8,128)S(1)}, f32[384,128]{1,0:T(8,128)}, u32[]{:S(2)}) copy-start(f32[384,128]{1,0:T(8,128)} %vsq_hbm.1) | copy-start | bytes 589828
  8.8 0.9 %copy-start.6 = (f32[128,384]{1,0:T(8,128)S(1)}, f32[128,384]{1,0:T(8,128)}, u32[]{:S(2)}) copy-start(f32[128,384]{1,0:T(8,128)} %omean_hbm.1) | copy-start | bytes 589828
  9.7 0.9 %copy-start.7 = (f32[128,384]{1,0:T(8,128)S(1)}, f32[128,384]{1,0:T(8,128)}, u32[]{:S(2)}) copy-start(f32[128,384]{1,0:T(8,128)} %osq_hbm.1) | copy-start | bytes 589828
  10.6 0.7 copy-start.8
  11.4 0.7 copy-start.9
  12.1 0.7 copy-start.10
  12.8 0.7 copy-start.11

commit v3 on v2

--- a/solution.py
+++ b/solution.py
@@ -518,18 +518,23 @@
             collective_id=0, has_side_effects=True, vmem_limit_bytes=32 * 1024 * 1024
         ),
     )(
-        block_input,
-        value_cotangent,
-        mixed_output,
-        output_cotangent,
-        value_basis,
-        output_basis,
-        value_weight,
-        output_weight.T,
-        value_mean,
-        value_square,
-        output_mean,
-        output_square,
+        *(
+            pltpu.with_memory_space_constraint(a, pltpu.HBM)
+            for a in (
+                block_input,
+                value_cotangent,
+                mixed_output,
+                output_cotangent,
+                value_basis,
+                output_basis,
+                value_weight,
+                output_weight.T,
+                value_mean,
+                value_square,
+                output_mean,
+                output_square,
+            )
+        )
     )
     out = pl.pallas_call(
         store,

time: 90 us -> 76.2 us (0.85)
  local copies, waits for them, and re-layouts: 12.9 us -> 0 us
    unnamed x24 -> x0, local copies, waits for them, and re-layouts: 12.9 us -> none
where the time goes in v3:
time: 76.2 us; the launch traced here: 76.1 us
  Pallas kernels  75.5 us (99%)
    pallas_call x1, Pallas kernels, on_device(): pl.pallas_call(functools.partial(kernel, scaling, entries), out_shape=sha...  74.1 us

profile of v3, /device:TPU:1, one launch (start us, length us, event | category | flops | bytes accessed | tf_op | source)
XLA Modules:
  0.0 76.1 jit_solution(5801132988541386894)
XLA Ops:
  0.6 74.1 %shard_map.195 = (f32[32,128]{1,0:T(8,128)S(1)}, bf16[2048,128]{1,0:T(8,128)(2,1)S(1)}, f32[32,128]{1,0:T(8,128)S(1)}, f32[384,128]{1,0:T(8,128)S(1)}, f32[384,1...) custom-call(bf16[1024,2048]{1,0:T(8,128)(2,1)} %x_hbm.1, ...), custom_call_target="tpu_custom_call" | custom-call | tf_op jit(solution)/shard_map/pallas_call | solution.py:482
  74.8 1.4 %shard_map.196 = (f32[32,128]{1,0:T(8,128)}, bf16[2048,128]{1,0:T(8,128)(2,1)}, f32[32,128]{1,0:T(8,128)}, f32[384,128]{1,0:T(8,128)}, f32[384,128]{1,0:T(8,128)...) custom-call(f32[32,128]{1,0:T(8,128)S(1)} %get-tuple-element.30.refs, ...), custom_call_target="tpu_custom_call" | custom-call | tf_op jit(solution)/shard_map/pallas_call | solution.py:539

commit v4 on v3

--- a/solution.py
+++ b/solution.py
@@ -16,7 +16,8 @@
 NEAR = (4, 12, 3, 13, 2, 14, 1, 15)
 IN_ORDER = (0, 1, 15, 2, 14, 3, 13, 4, 12, 5, 11, 6, 10, 7, 9, 8)
 RELAYED = {4: (4, 3, 2, 1), 12: (-3, -2, -1)}
-LAG_Y, LAG_X = 5, 9
+LAG_Y, LAG_X = 8, 14
+PRODUCTS = 8
 FAR_FIRST = (8, 7, 9, 6, 10, 5, 11, 4, 12, 3, 13, 2, 14, 1, 15)
 
 
@@ -70,6 +71,7 @@
     zrecv,
     lows,
     sums,
+    quarters,
     small,
     vstate,
     ostate,
@@ -93,6 +95,8 @@
     ay_r,
     cl_s,
     cl_r,
+    cy_s,
+    cy_r,
     wz_s,
     wz_r,
     wy_s,
@@ -138,11 +142,8 @@
             src_ref=src, dst_ref=dst, send_sem=ssem, recv_sem=rsem, device_id=device, device_id_type=MESH
         )
 
-    here = y * (NX * NC) + tp
-
-    def plane(j):
-        other = lax.rem(here + j, NY * NX * NC)
-        return {"fs": z * NY + other // (NX * NC), "tp": lax.rem(other, NX * NC)}
+    def tdev(j):
+        return {"fs": fs, "tp": lax.rem(tp + j, NX * NC)}
 
     half = rows // 2
 
@@ -172,28 +173,31 @@
     barrier = pltpu.get_barrier_semaphore()
     for j in NEAR:
         pl.semaphore_signal(barrier, inc=1, device_id=zdev(zup(j)), device_id_type=MESH)
-    for j in range(1, NY * NX * NC):
-        pl.semaphore_signal(barrier, inc=1, device_id=plane(j), device_id_type=MESH)
+    for j in range(1, NY):
+        pl.semaphore_signal(barrier, inc=1, device_id=ydev(yup(j)), device_id_type=MESH)
+    for j in range(1, NX * NC):
+        pl.semaphore_signal(barrier, inc=1, device_id=tdev(j), device_id_type=MESH)
 
     pltpu.make_async_copy(vb_hbm.at[part_of(0)], basis.at[c, fs, part_of(parity)], load_sem.at[0]).wait()
     pltpu.make_async_copy(vw_hbm, owned.at[0], load_sem.at[1]).wait()
     pltpu.make_async_copy(ow_hbm, owned.at[1], load_sem.at[8]).wait()
     weights[fs] = coded(owned[...])
 
-    pltpu.make_async_copy(v_hbm, vs, load_sem.at[2]).wait()
-    pltpu.make_async_copy(m_hbm, ms, load_sem.at[3]).wait()
+    pl.semaphore_wait(barrier, len(NEAR) + NY - 1 + NX * NC - 1)
+
     across = (((0,), (0,)), ((), ()))
-    for t in range(CHUNKS):
+
+    def gradient(k, t):
+        far, near, thin = ((x_hbm, xs, vs), (oc_hbm, ocs, ms))[k]
         at = pl.ds(t * size, size)
-        for k, (far, near, thin) in enumerate(((x_hbm, xs, vs), (oc_hbm, ocs, ms))):
-            pltpu.make_async_copy(far.at[at], near.at[at], chunk_sem.at[k, t]).wait()
-            part = lax.dot_general(thin[at, :], near[at, :], across, preferred_element_type=jnp.float32)
-            if t == 0:
-                grads[k] = part
-            else:
-                grads[k] += part
-
-    pl.semaphore_wait(barrier, len(NEAR) + NY * NX * NC - 1)
+        if t == 0:
+            pltpu.make_async_copy((v_hbm, m_hbm)[k], thin, load_sem.at[2 + k]).wait()
+        pltpu.make_async_copy(far.at[at], near.at[at], chunk_sem.at[k, t]).wait()
+        part = lax.dot_general(thin[at, :], near[at, :], across, preferred_element_type=jnp.float32)
+        if t == 0:
+            grads[k] = part
+        else:
+            grads[k] += part
 
     def relay(block_of, ssem, rsem):
         def down(d, to):
@@ -254,6 +258,8 @@
                     go(send_basis(d, to))
             for j in (2, 1, 3):
                 go(by(d, j))
+        if 0 <= s - PRODUCTS < 2 * CHUNKS:
+            gradient((s - PRODUCTS) % 2, (s - PRODUCTS) // 2)
         if 0 <= s - LAG_Y < NZ:
             d = IN_ORDER[s - LAG_Y]
             for j in range(1, NY):
@@ -359,18 +365,31 @@
 
     mine = lows[y].astype(jnp.float32)
     square = jnp.sum(mine * mine)
-    sums[here] = jnp.full((1, 128), square, jnp.float32)
+    sums[tp] = jnp.full((1, 128), square, jnp.float32)
 
     def cl(j):
-        block = sums.at[here]
-        return remote(block, block, cl_s.at[j - 1], cl_r.at[j - 1], plane(j))
+        block = sums.at[tp]
+        return remote(block, block, cl_s.at[j - 1], cl_r.at[j - 1], tdev(j))
 
     def cl_recv(j):
-        block = sums.at[lax.rem(here + NY * NX * NC - j, NY * NX * NC)]
-        return remote(block, block, cl_s.at[j - 1], cl_r.at[j - 1], plane(1))
-
-    for j in range(1, NY * NX * NC):
+        block = sums.at[lax.rem(tp + NX * NC - j, NX * NC)]
+        return remote(block, block, cl_s.at[j - 1], cl_r.at[j - 1], tdev(1))
+
+    def cy(j):
+        block = quarters.at[y]
+        return remote(block, block, cy_s.at[j - 1], cy_r.at[j - 1], ydev(yup(j)))
+
+    def cy_recv(j):
+        block = quarters.at[yup(NY - j)]
+        return remote(block, block, cy_s.at[j - 1], cy_r.at[j - 1], ydev(yup(1)))
+
+    for j in range(1, NX * NC):
         go(cl(j))
+    for j in range(1, NX * NC):
+        cl_recv(j).wait_recv()
+    quarters[y] = jnp.sum(sums[...], axis=0)
+    for j in (2, 1, 3):
+        go(cy(j))
     for j in (1, 3, 2):
         ay_recv(j).wait_recv()
     for k in range(2):
@@ -378,9 +397,9 @@
             for i in range(NZ // 2):
                 at = yy * quarter + i * piece
                 small[k, at : at + piece, :] = lows[yy, k * (NZ // 2) + i].astype(jnp.float32)
-    for j in range(1, NY * NX * NC):
-        cl_recv(j).wait_recv()
-    everyone = jnp.sum(sums[...], axis=0)
+    for j in range(1, NY):
+        cy_recv(j).wait_recv()
+    everyone = jnp.sum(quarters[...], axis=0)
     clip = 1.0 / jnp.sqrt(1.0 + everyone[:, 0:1] / entries)
 
     for i, (far, near) in enumerate(
@@ -466,7 +485,6 @@
     hbm = pl.BlockSpec(memory_space=pltpu.HBM)
     vmem = pl.BlockSpec(memory_space=pltpu.VMEM)
     dma = pltpu.SemaphoreType.DMA
-    near = NY * NX * NC - 1
     shapes = (
         jax.ShapeDtypeStruct((rows, local), f32),
         jax.ShapeDtypeStruct((width, local), bf16),
@@ -498,7 +516,8 @@
             pltpu.VMEM((NZ, piece, rank), f32),
             pltpu.VMEM((NZ - 1, piece, rank), f32),
             pltpu.VMEM((NY, NZ, piece, rank), bf16),
-            pltpu.VMEM((NY * NX * NC, 1, 128), f32),
+            pltpu.VMEM((NX * NC, 1, 128), f32),
+            pltpu.VMEM((NY, 1, 128), f32),
             pltpu.VMEM((2, local, rank), f32),
             pltpu.VMEM((2, rank, local), f32),
             pltpu.VMEM((2, local, rank), f32),
@@ -510,7 +529,8 @@
             *[dma((2, NY - 1))] * 2,
             *[dma((NZ - 1,))] * 4,
             *[dma((NY - 1,))] * 2,
-            *[dma((near,))] * 2,
+            *[dma((NX * NC - 1,))] * 2,
+            *[dma((NY - 1,))] * 2,
             *[dma((NZ - 1,))] * 2,
             *[dma((NZ, NY - 1))] * 2,
         ],

time: 76.2 us -> 71.9 us (0.944)
  Pallas kernels: 75.5 us -> 71.1 us
    pallas_call x1, Pallas kernels: 74.1 us -> 69.7 us  [on_device(): pl.pallas_call(functools.partial(kernel, scaling, entries), out_shape=sha...]
where the time goes in v4:
time: 71.9 us; the launch traced here: 71.7 us
  Pallas kernels  71.1 us (99%)
    pallas_call x1, Pallas kernels, on_device(): pl.pallas_call(functools.partial(kernel, scaling, entries), out_shape=sha...  69.7 us

profile of v4, /device:TPU:1, one launch (start us, length us, event | category | flops | bytes accessed | tf_op | source)
XLA Modules:
  0.0 71.7 jit_solution(6253721777240325622)
XLA Ops:
  0.6 69.7 %shard_map.195 = (f32[32,128]{1,0:T(8,128)S(1)}, bf16[2048,128]{1,0:T(8,128)(2,1)S(1)}, f32[32,128]{1,0:T(8,128)S(1)}, f32[384,128]{1,0:T(8,128)S(1)}, f32[384,1...) custom-call(bf16[1024,2048]{1,0:T(8,128)(2,1)} %x_hbm.1, ...), custom_call_target="tpu_custom_call" | custom-call | tf_op jit(solution)/shard_map/pallas_call | solution.py:500
  70.4 1.4 %shard_map.196 = (f32[32,128]{1,0:T(8,128)}, bf16[2048,128]{1,0:T(8,128)(2,1)}, f32[32,128]{1,0:T(8,128)}, f32[384,128]{1,0:T(8,128)}, f32[384,128]{1,0:T(8,128)...) custom-call(f32[32,128]{1,0:T(8,128)S(1)} %get-tuple-element.30.refs, ...), custom_call_target="tpu_custom_call" | custom-call | tf_op jit(solution)/shard_map/pallas_call | solution.py:559

commit v5 on v4

--- a/solution.py
+++ b/solution.py
@@ -16,7 +16,7 @@
 NEAR = (4, 12, 3, 13, 2, 14, 1, 15)
 IN_ORDER = (0, 1, 15, 2, 14, 3, 13, 4, 12, 5, 11, 6, 10, 7, 9, 8)
 RELAYED = {4: (4, 3, 2, 1), 12: (-3, -2, -1)}
-LAG_Y, LAG_X = 8, 14
+LAG_Y, LAG_X = 8, 16
 PRODUCTS = 8
 FAR_FIRST = (8, 7, 9, 6, 10, 5, 11, 4, 12, 3, 13, 2, 14, 1, 15)
 
@@ -238,13 +238,13 @@
         block = basis.at[c, pl.ds(zup(NZ - d if d else 0) * NY + w * pair, pair), part_of(1 - parity)]
         return remote(block, block, bx_s.at[d, w], bx_r.at[d, w], xdev(xup(1)))
 
-    def bd(d, w):
-        block = basis.at[c, pl.ds(zup(NZ - d if d else 0) * NY, NY), part_of(parity if w == 0 else 1 - parity)]
-        return remote(block, block, bd_s.at[d, w], bd_r.at[d, w], sibling)
-
-    def bd_recv(d, w):
-        block = basis.at[1 - c, pl.ds(zup(NZ - d if d else 0) * NY, NY), part_of(parity if w == 0 else 1 - parity)]
-        return remote(block, block, bd_s.at[d, w], bd_r.at[d, w], sibling)
+    def bd(d):
+        block = basis.at[c, pl.ds(zup(NZ - d if d else 0) * NY, NY)]
+        return remote(block, block, bd_s.at[d], bd_r.at[d], sibling)
+
+    def bd_recv(d):
+        block = basis.at[1 - c, pl.ds(zup(NZ - d if d else 0) * NY, NY)]
+        return remote(block, block, bd_s.at[d], bd_r.at[d], sibling)
 
     for to in NEAR:
         go(send_basis(0, to))
@@ -266,7 +266,6 @@
                 by_recv(d, j).wait_recv()
             for w in range(2):
                 go(bx(d, w))
-            go(bd(d, 0))
         if s == NZ:
             for to in NEAR:
                 go(send_weight(0, to))
@@ -274,7 +273,7 @@
             d = IN_ORDER[s - LAG_X]
             for w in range(2):
                 bx_recv(d, w).wait_recv()
-            go(bd(d, 1))
+            go(bd(d))
 
     def wy(d, j):
         block = weight_row(zup(NZ - d if d else 0))
@@ -284,12 +283,11 @@
         block = weights.at[zup(NZ - d if d else 0) * NY + yup(NY - j)]
         return remote(block, block, wy_s.at[d, j - 1], wy_r.at[d, j - 1], ydev(yup(1)))
 
-    for d in IN_ORDER:
-        for w in range(2):
-            bd_recv(d, w).wait_recv()
-
     quarter = local // NY
-    for k in range(2):
+    for turn, k in enumerate((c, 1 - c)):
+        if turn == 1:
+            for d in IN_ORDER:
+                bd_recv(d).wait_recv()
         whole = grads[k]
         high = whole.astype(jnp.bfloat16)
         low = (whole - high.astype(jnp.float32)).astype(jnp.bfloat16)
@@ -525,7 +523,8 @@
             dma((2, CHUNKS)),
             *[dma((NZ - 1,))] * 2,
             *[dma((NZ, NY - 1))] * 2,
-            *[dma((NZ, 2))] * 4,
+            *[dma((NZ, 2))] * 2,
+            *[dma((NZ,))] * 2,
             *[dma((2, NY - 1))] * 2,
             *[dma((NZ - 1,))] * 4,
             *[dma((NY - 1,))] * 2,

time: 71.9 us -> 68.9 us (0.958)
  Pallas kernels: 71.1 us -> 68.1 us
    pallas_call x1, Pallas kernels: 69.7 us -> 66.7 us  [on_device(): pl.pallas_call(functools.partial(kernel, scaling, entries), out_shape=sha...]
where the time goes in v5:
time: 68.9 us; the launch traced here: 68.8 us
  Pallas kernels  68.1 us (99%)
    pallas_call x1, Pallas kernels, on_device(): pl.pallas_call(functools.partial(kernel, scaling, entries), out_shape=sha...  66.7 us

profile of v5, /device:TPU:1, one launch (start us, length us, event | category | flops | bytes accessed | tf_op | source)
XLA Modules:
  0.0 68.8 jit_solution(14498933242854893791)
XLA Ops:
  0.6 66.7 %shard_map.195 = (f32[32,128]{1,0:T(8,128)S(1)}, bf16[2048,128]{1,0:T(8,128)(2,1)S(1)}, f32[32,128]{1,0:T(8,128)S(1)}, f32[384,128]{1,0:T(8,128)S(1)}, f32[384,1...) custom-call(bf16[1024,2048]{1,0:T(8,128)(2,1)} %x_hbm.1, ...), custom_call_target="tpu_custom_call" | custom-call | tf_op jit(solution)/shard_map/pallas_call | solution.py:498
  67.4 1.4 %shard_map.196 = (f32[32,128]{1,0:T(8,128)}, bf16[2048,128]{1,0:T(8,128)(2,1)}, f32[32,128]{1,0:T(8,128)}, f32[384,128]{1,0:T(8,128)}, f32[384,128]{1,0:T(8,128)...) custom-call(f32[32,128]{1,0:T(8,128)S(1)} %get-tuple-element.30.refs, ...), custom_call_target="tpu_custom_call" | custom-call | tf_op jit(solution)/shard_map/pallas_call | solution.py:558
